TPU v7x, 32 devices: a whole 2x2x4 slice. The times are simulated.
32 devices in a mesh: ep: 8 (over z, y), tp: 4 (over x, core).
Axes of the slice: x: 2, y: 2, z: 4, core: 2. Of those that a mesh axis runs over, the one named last changes fastest.
Arguments:
- tokens: bfloat16 [128, 1024], P('ep'), may hold values from -24 to 24
- seq_length: int32 [128], P('ep'), may hold values from 1024 to 16383
- ret_state: float32 [128, 4, 128, 256], P('ep', 'tp'), may hold values from -0.6 to 0.6
- norm_in: float32 [1024], replicated, may hold values from 0.1 to 1.9
- w_query: bfloat16 [1024, 512], P(None, 'tp'), may hold values from -0.1875 to 0.1875
- w_key: bfloat16 [1024, 512], P(None, 'tp'), may hold values from -0.1875 to 0.1875
- w_value: bfloat16 [1024, 1024], P(None, 'tp'), may hold values from -0.1875 to 0.1875
- head_gain: float32 [1024], P('tp'), may hold values from 0.1 to 1.9
- w_output: bfloat16 [1024, 1024], P('tp'), may hold values from -0.1875 to 0.1875
- norm_mid: float32 [1024], replicated, may hold values from 0.1 to 1.9
- route_expert: int32 [128, 2], P('ep'), may hold values from 0 to 3, all different within a row; in each aligned block of 16 rows (0 to 15, 16 to 31, ...) at most 12 rows name the same one
- route_score: float32 [128, 2], P('ep'), may hold values from -6 to 6
- expert_gate: bfloat16 [8, 1024, 1792], P('ep', None, 'tp'), may hold values from -0.1875 to 0.1875
- expert_up: bfloat16 [8, 1024, 1792], P('ep', None, 'tp'), may hold values from -0.1875 to 0.1875
- expert_down: bfloat16 [8, 1792, 1024], P('ep', 'tp'), may hold values from -0.09375 to 0.09375
Outputs:
- mixed: bfloat16 [128, 1024], P('ep', 'tp')
Inputs may be any that keep to these rules, and one draw needn't show every extreme that they name: `route_expert`: each row names 2 different experts; within the rows of one device no expert is named by more than 12 rows, and some device's rows name one expert exactly 12 times.
All inputs are finite; a program needn't handle non-finite values.
Results may differ from a plain program's by a relative error of at most 0.014.
Values may be sent and summed in bfloat16 or wider, within the bound.
A program may use at most 64 MiB of HBM per device.

v0:
```python
import jax
import jax.numpy as jnp
from jax import lax
from jax.sharding import PartitionSpec as P

DK = 128
DV = 256
SPREAD = 2
TOP_K = 2
EPS = 1e-06


def rotate(head_rows, positions):
    half_width = head_rows.shape[-1] // 2
    inverse = 10000.0 ** (-jnp.arange(half_width, dtype=jnp.float32) / half_width)
    angles = positions[:, None] * inverse[None, :]
    cosine = jnp.cos(angles)[:, None, :]
    sine_part = jnp.sin(angles)[:, None, :]
    first_half = head_rows[..., :half_width]
    second = head_rows[..., half_width:]
    return jnp.concatenate(
        [first_half * cosine - second * sine_part, first_half * sine_part + second * cosine],
        axis=-1,
    )


def body(
    tokens,
    seq_length,
    ret_state,
    norm_in,
    w_query,
    w_key,
    w_value,
    head_gain,
    w_output,
    norm_mid,
    route_expert,
    route_score,
    expert_gate,
    expert_up,
    expert_down,
):
    n_lanes = lax.axis_size("tp")
    n_groups = lax.axis_size("ep")
    lane_index = lax.axis_index("tp")
    local_rows = tokens.shape[0]
    width = tokens.shape[1]
    quarter = width // n_lanes
    heads_here = w_query.shape[1] // DK
    token_f = tokens.astype(jnp.float32)
    normed = (
        token_f * lax.rsqrt(jnp.mean(token_f * token_f, axis=-1, keepdims=True) + EPS) * norm_in
    ).astype(jnp.bfloat16)
    query_proj = jnp.dot(normed, w_query, preferred_element_type=jnp.float32).astype(jnp.bfloat16)
    key_proj = jnp.dot(normed, w_key, preferred_element_type=jnp.float32).astype(jnp.bfloat16)
    value_proj = jnp.dot(normed, w_value, preferred_element_type=jnp.float32).astype(jnp.bfloat16)
    positions = seq_length.astype(jnp.float32)
    q_rot = rotate(query_proj.astype(jnp.float32).reshape(local_rows, heads_here, DK), positions)
    k_rot = rotate(
        key_proj.astype(jnp.float32).reshape(local_rows, heads_here, DK), positions
    ) * DK ** (-0.5)
    value_rows = value_proj.astype(jnp.float32).reshape(local_rows, heads_here, DV)
    head_index = (lane_index * heads_here + jnp.arange(heads_here, dtype=jnp.int32)).astype(
        jnp.float32
    )
    decay_rate = 1.0 - jnp.exp2(-2.0 - 2.0 * head_index)
    carried = jnp.einsum("bhd,bhde->bhe", q_rot, ret_state, precision=lax.Precision.HIGHEST)
    within = jnp.sum(q_rot * k_rot, axis=-1, keepdims=True) * value_rows
    retained = decay_rate[None, :, None] * carried + within
    centre = jnp.mean(retained, axis=-1, keepdims=True)
    variance = jnp.mean(jnp.square(retained - centre), axis=-1, keepdims=True)
    ret_out = ((retained - centre) * lax.rsqrt(variance + EPS)).reshape(local_rows, heads_here * DV)
    ret_out = (ret_out * head_gain).astype(jnp.bfloat16)
    partial_value = jnp.dot(ret_out, w_output, preferred_element_type=jnp.float32)
    experts_n = n_groups // SPREAD
    cap = min(local_rows, max(2, 3 * local_rows * TOP_K // (2 * experts_n)))
    flat_rows = route_expert.reshape(-1)
    onehot = (flat_rows[:, None] == jnp.arange(experts_n, dtype=jnp.int32)[None, :]).astype(
        jnp.int32
    )
    rank_index = jnp.sum((jnp.cumsum(onehot, axis=0) - onehot) * onehot, axis=1)
    slot_index = flat_rows * cap + rank_index
    chosen_slot = (
        slot_index[:, None] == jnp.arange(experts_n * cap, dtype=jnp.int32)[None, :]
    ).astype(jnp.float32)
    chosen_slot = chosen_slot.reshape(local_rows, TOP_K, experts_n * cap)
    placing = jnp.sum(chosen_slot, axis=1).astype(jnp.bfloat16)
    weights = jax.nn.softmax(route_score, axis=-1)
    combine = jnp.sum(chosen_slot * weights[:, :, None], axis=1)
    gate_rows = expert_gate[0]
    up_rows = expert_up[0]
    down_rows = expert_down[0]
    attended = lax.psum(partial_value.astype(jnp.bfloat16), "tp").astype(jnp.float32)
    resid_full = (token_f + attended).astype(jnp.bfloat16)
    resid_f = resid_full.astype(jnp.float32)
    mid_full = (
        resid_f * lax.rsqrt(jnp.mean(resid_f * resid_f, axis=-1, keepdims=True) + EPS) * norm_mid
    ).astype(jnp.bfloat16)
    resid = lax.dynamic_slice_in_dim(resid_full, lane_index * quarter, quarter, 1)
    mid = lax.dynamic_slice_in_dim(mid_full, lane_index * quarter, quarter, 1)
    packed = jnp.einsum("re,rc->ec", placing, mid, preferred_element_type=jnp.float32).astype(
        jnp.bfloat16
    )
    packed = packed.reshape(experts_n, cap, quarter)
    send_buffer = jnp.repeat(packed, SPREAD, axis=0)
    received = lax.all_to_all(send_buffer, "ep", split_axis=0, concat_axis=0, tiled=True)
    groups, row_count, cols = received.shape
    piece_cols = lax.all_gather(received, "tp", axis=2, tiled=True)
    piece_width = piece_cols.shape[2]
    flat_in = piece_cols.reshape(groups * row_count, piece_width)
    gate_sum = jnp.dot(flat_in, gate_rows, preferred_element_type=jnp.float32)
    up_sum = jnp.dot(flat_in, up_rows, preferred_element_type=jnp.float32)
    hidden = (jax.nn.silu(gate_sum) * up_sum).astype(jnp.bfloat16)
    down_part = jnp.dot(hidden, down_rows, preferred_element_type=jnp.float32)
    share = lax.psum_scatter(
        down_part.astype(jnp.bfloat16), "tp", scatter_dimension=1, tiled=True
    ).astype(jnp.float32)
    returned = share.astype(jnp.bfloat16).reshape(groups, row_count, share.shape[1])
    arrived = lax.all_to_all(returned, "ep", split_axis=0, concat_axis=0, tiled=True)
    part_total = jnp.sum(
        arrived.reshape(experts_n, SPREAD, cap, quarter).astype(jnp.float32), axis=1
    )
    expert_out = part_total.astype(jnp.bfloat16)
    expert_mix = jnp.dot(
        combine,
        expert_out.reshape(experts_n * cap, quarter).astype(jnp.float32),
        precision=lax.Precision.HIGHEST,
    )
    return (resid.astype(jnp.float32) + expert_mix).astype(jnp.bfloat16)


def solution(mesh):
    placed = (
        P("ep", None),
        P("ep"),
        P("ep", "tp", None, None),
        P(),
        P(None, "tp"),
        P(None, "tp"),
        P(None, "tp"),
        P("tp"),
        P("tp", None),
        P(),
        P("ep", None),
        P("ep", None),
        P("ep", None, "tp"),
        P("ep", None, "tp"),
        P("ep", "tp", None),
    )
    return jax.shard_map(body, mesh=mesh, in_specs=placed, out_specs=P("ep", "tp"), check_vma=False)
```

profile of v0, /device:TPU:0, one launch (start us, length us, event | category | flops | bytes accessed | tf_op | source)
XLA Modules:
  0.0 89.4 jit_solution(11786482664120521328)
XLA Ops:
  6.7 0.8 reduce_max.9
  7.5 0.7 fusion.51
  8.2 0.7 fusion.50
  8.9 0.7 convert_element_type.79
  9.5 0.9 fusion.22
  10.4 1.2 %fusion.10 = f32[16,1,128]{2,0,1:T(8,128)S(1)} fusion(bf16[1024,128]{1,0:T(8,128)(2,1)} %param.20, bf16[16,1024]{1,0:T(8,128)(2,1)} %param.15, f32[1024]{0:T(1024)} %param.18, f32[16]{0:T(128)S(1)} %add_rsqrt_fusion.2), kind=kOutput, calls=%fused_computation.18 | convolution fusion | flops 4263936 | bytes 307264 | tf_op jit(solution)/shard_map/dot_general | solution.py:56
  11.6 1.2 %fusion.8 = f32[16,1,128]{2,0,1:T(8,128)S(1)} fusion(bf16[1024,128]{1,0:T(8,128)(2,1)} %param.19, bf16[16,1024]{1,0:T(8,128)(2,1)} %param.15, f32[1024]{0:T(1024)} %param.18, f32[16]{0:T(128)S(1)} %add_rsqrt_fusion.2), kind=kOutput, calls=%fused_computation.16 | convolution fusion | flops 4263936 | bytes 307264 | tf_op jit(solution)/shard_map/dot_general | solution.py:55
  12.8 0.8 copy.28
  13.8 0.2 fusion.45
  14.0 1.1 %fusion = f32[16,1,256]{2,1,0:T(1,128)S(1)} fusion(f32[16,128,1]{1,2,0:T(1,128)S(1)} %bitcast.45, f32[16,1,128,256]{3,2,1,0:T(8,128)S(1)} %copy-done), kind=kOutput, calls=%fused_computation | convolution fusion | flops 6291456 | bytes 2121728 | tf_op jit(solution)/shard_map/bhd,bhde->bhe/dot_general | solution.py:68
  15.2 0.3 fusion.58
  15.5 0.2 multiply_reduce_fusion.1
  15.7 0.2 convolution_convert_fusion.1
  15.9 12.9 %psum.7 = bf16[16,1024]{1,0:T(8,128)(2,1)S(1)} all-reduce(bf16[16,1024]{1,0:T(8,128)(2,1)S(1)} %convolution_convert_fusion.1), channel_id=1, replica_groups=mesh['ep'=8,'tp'=4] {'tp'}, use_global_device_ids=true, to_apply=%region_4.0 | all-reduce | flops 16384 | bytes 65536 | tf_op jit(solution)/shard_map/psum | solution.py:94
  29.1 0.2 select_reduce_fusion.1
  29.5 0.8 dynamic-slice
  30.6 12.5 %all_to_all.10 = bf16[8,12,256]{2,1,0:T(8,128)(2,1)S(1)} all-to-all(bf16[8,12,256]{2,1,0:T(8,128)(2,1)S(1)} %bitcast.44), channel_id=1, replica_groups=mesh['ep'=8,'tp'=4] {'ep'}, dimensions={0} | all-to-all | bytes 98304 | tf_op jit(solution)/shard_map/all_to_all | solution.py:107
  43.1 5.8 %all_gather.3 = bf16[8,12,1024]{2,1,0:T(8,128)(2,1)S(1)} all-gather(bf16[8,12,256]{2,1,0:T(8,128)(2,1)S(1)} %all_to_all.10), channel_id=1, replica_groups=mesh['ep'=8,'tp'=4] {'tp'}, dimensions={2}, use_global_device_ids=true | all-gather | bytes 245760 | tf_op jit(solution)/shard_map/all_gather | solution.py:109
  48.9 0.4 fusion.14
  49.4 2.8 %convolution_convert_fusion = bf16[96,1024]{1,0:T(8,128)(2,1)} fusion(bf16[96,1024]{1,0:T(8,128)(2,1)S(1)} %reshape.273, bf16[1,448,1024]{2,1,0:T(8,128)(2,1)} %param.29, bf16[1,1024,448]{1,2,0:T(8,128)(2,1)} %param.28, f32[96,448]{1,0:T(8,128)S(1)} %fusion.14), kind=kOutput, calls=%fused_computation.2 | convolution fusion | flops 176517120 | bytes 2400256 | tf_op jit(solution)/shard_map/dot_general | solution.py:115
  52.2 16.5 %reduce-scatter.2.cloned.1.call-done = bf16[96,256]{1,0:T(8,128)(2,1)} async-done(((bf16[96,1024]{1,0:T(8,128)(2,1)}), bf16[96,256]{1,0:T(8,128)(2,1)}) %reduce-scatter.2.cloned.1.call-update) | async-done | bytes 49168 | tf_op jit(solution)/shard_map/reduce_scatter | solution.py:116
  68.7 0.8 reshape.274
  69.5 12.2 %all_to_all.11 = bf16[8,12,256]{2,1,0:T(8,128)(2,1)S(1)} all-to-all(bf16[8,12,256]{2,1,0:T(8,128)(2,1)S(1)} %reshape.274), channel_id=1, replica_groups=mesh['ep'=8,'tp'=4] {'ep'}, dimensions={0} | all-to-all | bytes 98304 | tf_op jit(solution)/shard_map/all_to_all | solution.py:120
  81.8 0.7 fusion.3
  (39 shorter events, 1.1 us)
Async XLA Ops:
  6.5 7.5 %copy-start = (f32[16,1,128,256]{3,2,1,0:T(8,128)S(1)}, f32[16,1,128,256]{3,2,1,0:T(8,128)}, u32[]{:S(2)}) copy-start(f32[16,1,128,256]{3,2,1,0:T(8,128)} %param.17) | copy-start | bytes 6291460
  6.5 8.6 %copy-start.3 = (bf16[16,1024]{1,0:T(8,128)(2,1)S(1)}, bf16[16,1024]{1,0:T(8,128)(2,1)}, u32[]{:S(2)}) copy-start(bf16[16,1024]{1,0:T(8,128)(2,1)} %param.15) | copy-start | bytes 98308
  6.5 8.6 %copy-start.7 = (f32[1024]{0:T(1024)S(1)}, f32[1024]{0:T(1024)}, u32[]{:S(2)}) copy-start(f32[1024]{0:T(1024)} %param.18) | copy-start | bytes 12292
  6.5 9.2 %copy-start.5 = (f32[256]{0:T(256)S(1)}, f32[256]{0:T(256)}, u32[]{:S(2)}) copy-start(f32[256]{0:T(256)} %param.22) | copy-start | bytes 3076
  6.5 62.2 %reduce-scatter.2.cloned.1.call-start = ((), (), s32[]{:S(2)}) async-start(), calls=%async_computation.3 | async-start | bytes 245760 | tf_op jit(solution)/shard_map/reduce_scatter | solution.py:116
  10.4 19.1 %copy-start.4 = (s32[16,2]{0,1:T(2,128)S(1)}, s32[16,2]{0,1:T(2,128)}, u32[]{:S(2)}) copy-start(s32[16,2]{0,1:T(2,128)} %param.25) | copy-start | bytes 388
  13.7 1.5 %copy-start.6 = (bf16[1024,256]{1,0:T(8,128)(2,1)S(1)}, bf16[1024,256]{1,0:T(8,128)(2,1)}, u32[]{:S(2)}) copy-start(bf16[1024,256]{1,0:T(8,128)(2,1)} %param.21) | copy-start | bytes 1572868
  13.7 2.0 %copy-start.2 = (bf16[256,1024]{1,0:T(8,128)(2,1)S(1)}, bf16[256,1024]{1,0:T(8,128)(2,1)}, u32[]{:S(2)}) copy-start(bf16[256,1024]{1,0:T(8,128)(2,1)} %param.23) | copy-start | bytes 1572868
  14.0 34.9 %copy-start.1 = (bf16[1,1024,448]{1,2,0:T(8,128)(2,1)S(1)}, bf16[1,1024,448]{1,2,0:T(8,128)(2,1)}, u32[]{:S(2)}) copy-start(bf16[1,1024,448]{1,2,0:T(8,128)(2,1)} %param.27) | copy-start | bytes 2752516
Sparse Core Ops, SparseCore 0:
  52.3 16.3 reduce-scatter.1
where the time goes:
time: 89.9 us; the launch traced here: 89.4 us
  blocking collectives  43.4 us (48%)
  waiting for transfers between devices  16.5 us (18%)
  between operations  13.6 us (15%)
  matrix products  8.21 us (9%)
  other arithmetic  4.82 us (5%)
  local copies, waits for them, and re-layouts  2.74 us (3%)
    reduce_scatter x1, waiting for transfers between devices, body(): lax.psum_scatter(down_part.astype(jnp.bfloat16), 'tp', scatter_dimension=...  16.5 us
    psum x1, blocking collectives, body(): lax.psum(partial_value.astype(jnp.bfloat16), 'tp').astype(jnp.float32)  12.9 us
    all_to_all x1, blocking collectives, body(): lax.all_to_all(send_buffer, 'ep', split_axis=0, concat_axis=0, tiled=True)  12.5 us
    all_to_all x1, blocking collectives, body(): lax.all_to_all(returned, 'ep', split_axis=0, concat_axis=0, tiled=True)  12.2 us
    all_gather x1, blocking collectives, body(): piece_cols = lax.all_gather(received, 'tp', axis=2, tiled=True)  5.76 us
    dot_general x1, matrix products, body(): down_part = jnp.dot(hidden, down_rows, preferred_element_type=jnp.float32)  2.82 us
  transfers between devices with their start and end apart: 1, of which 1 were waited for; matrix products, arithmetic and copies ran while one was open for 0% of the time, Pallas kernels for 0%

commit v1 on v0

--- a/solution.py
+++ b/solution.py
@@ -8,6 +8,12 @@
 SPREAD = 2
 TOP_K = 2
 EPS = 1e-06
+
+
+def gather_and_add(x, axis):
+    pieces = lax.all_gather(x, axis, axis=0, tiled=False)
+    acc = pieces.sum(axis=0)
+    return acc
 
 
 def rotate(head_rows, positions):
@@ -91,7 +97,7 @@
     gate_rows = expert_gate[0]
     up_rows = expert_up[0]
     down_rows = expert_down[0]
-    attended = lax.psum(partial_value.astype(jnp.bfloat16), "tp").astype(jnp.float32)
+    attended = gather_and_add(partial_value.astype(jnp.bfloat16), "tp").astype(jnp.float32)
     resid_full = (token_f + attended).astype(jnp.bfloat16)
     resid_f = resid_full.astype(jnp.float32)
     mid_full = (

time: 89.9 us -> 96.2 us (1.070)
  other arithmetic: 4.82 us -> 11.8 us
  blocking collectives: 43.4 us -> 37.4 us
  local copies, waits for them, and re-layouts: 2.74 us -> 6.26 us
  waiting for transfers between devices: 16.5 us -> 17.5 us
    psum x1 -> x0, blocking collectives: 12.9 us -> none  [body(): lax.psum(partial_value.astype(jnp.bfloat16), 'tp').astype(jnp.float32)]
    all_gather x0 -> x1, blocking collectives: none -> 6.51 us  [gather_and_add(): pieces = lax.all_gather(x, axis, axis=0, tiled=False)]
    reduce_sum x2, local copies, waits for them, and re-layouts: 0.17 us -> 2.64 us  [body(): rank_index = jnp.sum((jnp.cumsum(onehot, axis=0) - onehot) * onehot, axis=1)]
    another operation x1, other arithmetic: 0.06 us -> 1.35 us  [body(): rank_index = jnp.sum((jnp.cumsum(onehot, axis=0) - onehot) * onehot, axis=1)]
    add x1, other arithmetic: 0.01 us -> 1.25 us  [body(): slot_index = flat_rows * cap + rank_index]
    reduce_sum x1, other arithmetic: 0.18 us -> 1.41 us  [body(): rank_index = jnp.sum((jnp.cumsum(onehot, axis=0) - onehot) * onehot, axis=1)]
where the time goes in v1:
time: 96.2 us; the launch traced here: 95.4 us
  blocking collectives  37.4 us (39%)
  waiting for transfers between devices  17.5 us (18%)
  between operations  13.6 us (14%)
  other arithmetic  11.8 us (12%)
  matrix products  8.87 us (9%)
  local copies, waits for them, and re-layouts  6.26 us (7%)
    reduce_scatter x1, waiting for transfers between devices, body(): lax.psum_scatter(down_part.astype(jnp.bfloat16), 'tp', scatter_dimension=...  17.5 us
    all_to_all x1, blocking collectives, body(): lax.all_to_all(send_buffer, 'ep', split_axis=0, concat_axis=0, tiled=True)  12.9 us
    all_to_all x1, blocking collectives, body(): lax.all_to_all(returned, 'ep', split_axis=0, concat_axis=0, tiled=True)  12.2 us
    all_gather x1, blocking collectives, gather_and_add(): pieces = lax.all_gather(x, axis, axis=0, tiled=False)  6.51 us
    all_gather x1, blocking collectives, body(): piece_cols = lax.all_gather(received, 'tp', axis=2, tiled=True)  5.76 us
    dot_general x1, matrix products, body(): down_part = jnp.dot(hidden, down_rows, preferred_element_type=jnp.float32)  2.81 us
    reduce_sum x2, local copies, waits for them, and re-layouts, body(): rank_index = jnp.sum((jnp.cumsum(onehot, axis=0) - onehot) * onehot, axis=1)  2.64 us
  transfers between devices with their start and end apart: 1, of which 1 were waited for; matrix products, arithmetic and copies ran while one was open for 0% of the time, Pallas kernels for 0%

profile of v1, /device:TPU:0, one launch (start us, length us, event | category | flops | bytes accessed | tf_op | source)
XLA Modules:
  0.0 95.4 jit_solution(1410387260833597594)
XLA Ops:
  6.6 0.8 reduce_max.9
  8.2 1.3 %fusion.50 = f32[16,2]{0,1:T(2,128)} fusion(f32[16,2]{0,1:T(2,128)} %param.26, f32[16]{0:T(128)S(1)} %fusion.51, f32[16]{0:T(128)S(1)} %reduce_max.9), kind=kLoop, calls=%fused_computation.76 | loop fusion | flops 64 | bytes 384 | tf_op jit(solution)/shard_map/div | solution.py:95
  10.1 0.9 fusion.22
  11.0 1.2 %fusion.10 = f32[16,1,128]{2,0,1:T(8,128)S(1)} fusion(bf16[1024,128]{1,0:T(8,128)(2,1)} %param.20, bf16[16,1024]{1,0:T(8,128)(2,1)} %param.15, f32[1024]{0:T(1024)} %param.18, f32[16]{0:T(128)S(1)} %add_rsqrt_fusion.2), kind=kOutput, calls=%fused_computation.18 | convolution fusion | flops 4263936 | bytes 307264 | tf_op jit(solution)/shard_map/dot_general | solution.py:62
  12.1 1.2 %fusion.8 = f32[16,1,128]{2,0,1:T(8,128)S(1)} fusion(bf16[1024,128]{1,0:T(8,128)(2,1)} %param.19, bf16[16,1024]{1,0:T(8,128)(2,1)} %param.15, f32[1024]{0:T(1024)} %param.18, f32[16]{0:T(128)S(1)} %add_rsqrt_fusion.2), kind=kOutput, calls=%fused_computation.16 | convolution fusion | flops 4263936 | bytes 307264 | tf_op jit(solution)/shard_map/dot_general | solution.py:61
  13.3 0.8 copy.28
  15.1 1.1 %fusion = f32[16,1,256]{2,1,0:T(1,128)S(1)} fusion(f32[16,128,1]{1,2,0:T(1,128)S(1)} %bitcast.47, f32[16,1,128,256]{3,2,1,0:T(8,128)S(1)} %copy-done), kind=kOutput, calls=%fused_computation | convolution fusion | flops 6291456 | bytes 2121728 | tf_op jit(solution)/shard_map/bhd,bhde->bhe/dot_general | solution.py:74
  18.5 1.4 %reduce_window_sum.11 = s32[32,4]{1,0:T(8,128)} reduce-window(s32[32,4]{1,0:T(8,128)} %fusion.28, s32[]{:T(128)} %constant.51.clone.1), window={size=32x1 pad=31_0x0_0}, to_apply=%region_5.6 | reduce-window | flops 3968 | bytes 1028 | tf_op jit(solution)/shard_map/jit(cumsum)/reduce_window_sum | solution.py:88
  19.9 1.4 %select_reduce_fusion.1 = s32[32]{0:T(128)} fusion(s32[32,4]{1,0:T(8,128)} %reduce_window_sum.11, s32[32]{0:T(128)} %eq.29), kind=kLoop, calls=%fused_computation.45 | loop fusion | flops 608 | bytes 768 | tf_op jit(solution)/shard_map/reduce_sum | solution.py:88
  21.3 1.3 %reduce_sum.113 = s32[16,2]{1,0:T(8,128)} reshape(s32[32]{0:T(128)} %select_reduce_fusion.1) | data formatting | bytes 256 | tf_op jit(solution)/shard_map/reduce_sum | solution.py:88
  22.6 1.4 %copy.29 = s32[16,2]{0,1:T(2,128)} copy(s32[16,2]{1,0:T(8,128)} %reduce_sum.113) | data formatting | bytes 256 | tf_op jit(solution)/shard_map/reduce_sum | solution.py:88
  23.9 1.2 %multiply_add_fusion = s32[16,2]{0,1:T(2,128)} fusion(s32[16,2]{0,1:T(2,128)} %copy.29, s32[16,2]{0,1:T(2,128)} %param.25), kind=kLoop, calls=%fused_computation.75 | loop fusion | flops 64 | bytes 384 | tf_op jit(solution)/shard_map/add | solution.py:89
  25.2 0.9 convolution_convert_fusion.1
  26.1 6.5 %all-gather = bf16[64,1024]{1,0:T(8,128)(2,1)S(1)} all-gather(bf16[16,1024]{1,0:T(8,128)(2,1)S(1)} %convolution_convert_fusion.1), channel_id=2, replica_groups=mesh['ep'=8,'tp'=4] {'tp'}, dimensions={0}, use_global_device_ids=true | all-gather | bytes 163840 | tf_op jit(solution)/shard_map/all_gather | solution.py:14
  32.6 0.9 multiply_reduce_fusion
  33.5 0.8 dynamic-slice
  34.3 0.8 convert_reduce_fusion
  35.3 12.9 %all_to_all.10 = bf16[8,12,256]{2,1,0:T(8,128)(2,1)S(1)} all-to-all(bf16[8,12,256]{2,1,0:T(8,128)(2,1)S(1)} %bitcast.46), channel_id=1, replica_groups=mesh['ep'=8,'tp'=4] {'ep'}, dimensions={0} | all-to-all | bytes 98304 | tf_op jit(solution)/shard_map/all_to_all | solution.py:113
  48.2 5.8 %all_gather.11 = bf16[8,12,1024]{2,1,0:T(8,128)(2,1)S(1)} all-gather(bf16[8,12,256]{2,1,0:T(8,128)(2,1)S(1)} %all_to_all.10), channel_id=1, replica_groups=mesh['ep'=8,'tp'=4] {'tp'}, dimensions={2}, use_global_device_ids=true | all-gather | bytes 245760 | tf_op jit(solution)/shard_map/all_gather | solution.py:115
  54.5 2.8 %convolution_convert_fusion = bf16[96,1024]{1,0:T(8,128)(2,1)} fusion(bf16[96,1024]{1,0:T(8,128)(2,1)S(1)} %reshape.273, bf16[1,448,1024]{2,1,0:T(8,128)(2,1)} %param.29, bf16[1,1024,448]{1,2,0:T(8,128)(2,1)} %param.28, f32[96,448]{1,0:T(8,128)S(1)} %fusion.14), kind=kOutput, calls=%fused_computation.2 | convolution fusion | flops 176517120 | bytes 2400256 | tf_op jit(solution)/shard_map/dot_general | solution.py:121
  57.3 17.5 %reduce-scatter.2.cloned.1.call-done = bf16[96,256]{1,0:T(8,128)(2,1)} async-done(((bf16[96,1024]{1,0:T(8,128)(2,1)}), bf16[96,256]{1,0:T(8,128)(2,1)}) %reduce-scatter.2.cloned.1.call-update) | async-done | bytes 49168 | tf_op jit(solution)/shard_map/reduce_scatter | solution.py:122
  74.8 0.8 reshape.274
  75.6 12.2 %all_to_all.11 = bf16[8,12,256]{2,1,0:T(8,128)(2,1)S(1)} all-to-all(bf16[8,12,256]{2,1,0:T(8,128)(2,1)S(1)} %reshape.274), channel_id=1, replica_groups=mesh['ep'=8,'tp'=4] {'ep'}, dimensions={0} | all-to-all | bytes 98304 | tf_op jit(solution)/shard_map/all_to_all | solution.py:126
  87.8 0.7 fusion.3
  (44 shorter events, 5.4 us)
Async XLA Ops:
  6.5 8.5 %copy-start = (f32[16,1,128,256]{3,2,1,0:T(8,128)S(1)}, f32[16,1,128,256]{3,2,1,0:T(8,128)}, u32[]{:S(2)}) copy-start(f32[16,1,128,256]{3,2,1,0:T(8,128)} %param.17) | copy-start | bytes 6291460
  6.5 18.7 %copy-start.2 = (bf16[256,1024]{1,0:T(8,128)(2,1)S(1)}, bf16[256,1024]{1,0:T(8,128)(2,1)}, u32[]{:S(2)}) copy-start(bf16[256,1024]{1,0:T(8,128)(2,1)} %param.23) | copy-start | bytes 1572868
  6.5 68.2 %reduce-scatter.2.cloned.1.call-start = ((), (), s32[]{:S(2)}) async-start(), calls=%async_computation.3 | async-start | bytes 245760 | tf_op jit(solution)/shard_map/reduce_scatter | solution.py:122
  11.0 1.2 %copy-start.8 = (f32[16]{0:T(128)}, f32[16]{0:T(128)S(1)}, u32[]{:S(2)}) copy-start(f32[16]{0:T(128)S(1)} %add_rsqrt_fusion.2) | copy-start | bytes 196
  14.7 1.5 %copy-start.3 = (bf16[16,1024]{1,0:T(8,128)(2,1)S(1)}, bf16[16,1024]{1,0:T(8,128)(2,1)}, u32[]{:S(2)}) copy-start(bf16[16,1024]{1,0:T(8,128)(2,1)} %param.15) | copy-start | bytes 98308
  14.7 1.5 %copy-start.6 = (bf16[1024,256]{1,0:T(8,128)(2,1)S(1)}, bf16[1024,256]{1,0:T(8,128)(2,1)}, u32[]{:S(2)}) copy-start(bf16[1024,256]{1,0:T(8,128)(2,1)} %param.21) | copy-start | bytes 1572868
  14.7 1.5 %copy-start.7 = (f32[1024]{0:T(1024)S(1)}, f32[1024]{0:T(1024)}, u32[]{:S(2)}) copy-start(f32[1024]{0:T(1024)} %param.18) | copy-start | bytes 12292
  14.7 1.5 %copy-start.9 = (f32[16]{0:T(128)S(1)}, f32[16]{0:T(128)}, u32[]{:S(2)}) copy-start(f32[16]{0:T(128)} %copy-done.8) | copy-start | bytes 196
  14.7 3.1 %copy-start.4 = (s32[32]{0:T(128)S(1)}, s32[32]{0:T(128)}, u32[]{:S(2)}) copy-start(s32[32]{0:T(128)} %eq.29) | copy-start | bytes 388
  15.1 39.0 %copy-start.1 = (bf16[1,1024,448]{1,2,0:T(8,128)(2,1)S(1)}, bf16[1,1024,448]{1,2,0:T(8,128)(2,1)}, u32[]{:S(2)}) copy-start(bf16[1,1024,448]{1,2,0:T(8,128)(2,1)} %param.27) | copy-start | bytes 2752516
  16.5 0.5 copy-start.5
Sparse Core Ops, SparseCore 0:
  57.4 17.3 reduce-scatter.1
